TPU v7x, 32 devices: a whole 2x2x4 slice. The times are simulated.
32 devices in a mesh: sp: 8 (over z, y), dp: 4 (over x, core).
Axes of the slice: x: 2, y: 2, z: 4, core: 2. Of those that a mesh axis runs over, the one named last changes fastest.
Arguments:
- query_first: bfloat16 [4, 1024, 1024], P('dp', 'sp'), may hold values from -200 to 200
- key_first: bfloat16 [4, 1024, 1024], P('dp', 'sp'), may hold values from -8 to 8
- query_second: bfloat16 [4, 1024, 1024], P('dp', 'sp'), may hold values from -200 to 200
- key_second: bfloat16 [4, 1024, 1024], P('dp', 'sp'), may hold values from -8 to 8
- value_rows: bfloat16 [4, 1024, 2048], P('dp', 'sp'), may hold values from -6 to 6
- mix_lambda: float32 [16], replicated, may hold values from 0.3 to 0.8
- head_gain: float32 [128], replicated, may hold values from 0.1 to 1.9
- residual: bfloat16 [4, 1024, 2048], P('dp', 'sp'), may hold values from -6 to 6
- out_weight: bfloat16 [2048, 2048], replicated, may hold values from -0.125 to 0.125
- norm_gain: float32 [2048], replicated, may hold values from 0.1 to 1.9
- routes: int32 [4, 1024, 4], P('dp', 'sp'), may hold values from 0 to 31, all different within a row; in each aligned block of 128 rows (0 to 127, 128 to 255, ..., all dimensions but the last counted through in order) at most 24 rows name the same one
- route_weights: float32 [4, 1024, 4], P('dp', 'sp'), may hold values from 0.1 to 1
- gate_weight: bfloat16 [32, 2048, 1024], P(('sp', 'dp')), may hold values from -0.375 to 0.375
- up_weight: bfloat16 [32, 2048, 1024], P(('sp', 'dp')), may hold values from -0.375 to 0.375
- down_weight: bfloat16 [32, 1024, 2048], P(('sp', 'dp')), may hold values from -0.046875 to 0.046875
Outputs:
- layer_out: bfloat16 [4, 1024, 2048], P('dp', 'sp')
Inputs may be any that keep to these rules, and one draw needn't show every extreme that they name: `routes`: within the rows of one device (aligned blocks of 128 positions of a sequence) no expert is named more than 24 times, a bound that some block reaches.
All inputs are finite; a program needn't handle non-finite values.
Results may differ from a plain program's by a relative error of at most 0.0075.
Values may be sent and summed in bfloat16 or wider, within the bound.
A program may use at most 128 MiB of HBM per device.

v0:
```python
import functools

import jax
import jax.numpy as jnp
from jax import lax
from jax.experimental import pallas as pl
from jax.experimental.pallas import tpu as pltpu
from jax.sharding import PartitionSpec as P

MESH = pl.DeviceIdType.MESH
VMEM = pltpu.VMEM
F32 = jnp.float32
BF16 = jnp.bfloat16


def vspec(number):
    return [pl.BlockSpec(memory_space=VMEM)] * number


def greet(peers):
    barrier = pltpu.get_barrier_semaphore()
    for peer in peers:
        pl.semaphore_signal(barrier, inc=1, device_id=peer, device_id_type=MESH)
    pl.semaphore_wait(barrier, len(peers))


def remote(src, dst, send_sem, recv_sem, peer):
    return pltpu.make_async_remote_copy(
        src_ref=src, dst_ref=dst, send_sem=send_sem, recv_sem=recv_sem, device_id=peer, device_id_type=MESH
    )


def attention_kernel(
    n, rows, heads_local, hd, hv, sliced,
    lam_ref, gain_ref, q1, k1, q2, k2, vv, meta,
    out_ref, meta_out,
    b_q1, b_k1, b_q2, b_k2, b_v, obuf, prob, mix,
    send_sem, recv_sem, local_sem, osend, orecv,
):
    me, dp = lax.axis_index("sp"), lax.axis_index("dp")
    ins = (k1, k2, q1, q2, vv)
    bufs = (b_k1, b_k2, b_q1, b_q2, b_v)
    peers = [(lax.rem(me + d, n), dp) for d in range(1, n)]
    greet(peers)

    def part(index, j):
        if not sliced[index]:
            return ins[index].at[j]
        width = bufs[index].shape[2]
        return ins[index].at[:, pl.ds(pl.multiple_of(j * width, 128), width)]

    def move(index, d):
        j = lax.rem(me + d, n)
        if index == 5:
            return remote(meta, meta_out.at[me], send_sem.at[5, d], recv_sem.at[5, me], (j, dp))
        return remote(part(index, j), bufs[index].at[me], send_sem.at[index, d], recv_sem.at[index, me], (j, dp))

    order = (0, 2, 1, 3, 4, 5)
    sends = [move(index, d) for index in order for d in range(1, n)]
    for copy in sends:
        copy.start()
    locals_ = [pltpu.make_async_copy(part(i, me), bufs[i].at[me], local_sem.at[i]) for i in range(5)]
    locals_.append(pltpu.make_async_copy(meta, meta_out.at[me], local_sem.at[5]))
    for copy in locals_:
        copy.start()
    for copy in locals_:
        copy.wait()

    def arrived(index):
        for d in range(1, n):
            j = lax.rem(me + d, n)
            if index == 5:
                remote(meta, meta_out.at[j], send_sem.at[5, d], recv_sem.at[5, j], (j, dp)).wait_recv()
            else:
                remote(
                    part(index, j), bufs[index].at[j], send_sem.at[index, d], recv_sem.at[index, j], (j, dp)
                ).wait_recv()

    group = 2 if n % 2 == 0 else 1
    qb = group * rows
    width = heads_local * hd
    lw = heads_local * hv
    lane = lax.broadcasted_iota(jnp.int32, (1, width), 1) // hd
    scale = hd ** (-0.5)
    blocks = [(i * group, (i + 1) * group) for i in reversed(range(n // group))]

    def softs(bq, bk, use):
        for lo, hi in blocks:
            keys = hi * rows
            visible = lax.broadcasted_iota(jnp.int32, (qb, keys), 1) <= lo * rows + lax.broadcasted_iota(
                jnp.int32, (qb, keys), 0
            )
            for h in range(heads_local):
                query = bq[lo:hi].reshape(qb, width)
                query = jnp.where(lane == h, query, jnp.zeros_like(query))
                key = bk[:hi].reshape(keys, width)
                score = lax.dot_general(query, key, (((1,), (1,)), ((), ())), preferred_element_type=F32) * scale
                score = jnp.where(visible, score, -1e30)
                powers = jnp.exp(score - jnp.max(score, axis=-1, keepdims=True))
                use(h, slice(lo * rows, hi * rows), keys, powers, jnp.sum(powers, axis=-1, keepdims=True))

    def first(h, at, keys, powers, total):
        prob[h, at, :keys] = powers * (1.0 / total)

    def second(h, at, keys, powers, total):
        mix[h, at, :keys] = (prob[h, at, :keys] - powers * (lam_ref[h] / total)).astype(BF16)

    arrived(0)
    arrived(2)
    softs(b_q1, b_k1, first)
    arrived(1)
    arrived(3)
    softs(b_q2, b_k2, second)
    arrived(4)
    arrived(5)
    for lo, hi in blocks:
        keys = hi * rows
        for h in range(heads_local):
            value = b_v[:hi, :, h * hv : (h + 1) * hv].reshape(keys, hv)
            raw = jnp.dot(mix[h, lo * rows : hi * rows, :keys], value, preferred_element_type=F32)
            factor = lax.rsqrt(jnp.mean(raw * raw, axis=-1, keepdims=True) + 1e-06)
            done = (raw * factor * gain_ref[...]).astype(BF16)
            obuf[lo:hi, :, h * hv : (h + 1) * hv] = done.reshape(group, rows, hv)
        for j in range(lo, hi):

            @pl.when(j != me)
            def _(j=j):
                remote(
                    obuf.at[j],
                    out_ref.at[:, pl.ds(pl.multiple_of(me * lw, 128), lw)],
                    osend.at[j], orecv.at[me], (j, dp),
                ).start()

    out_ref[:, pl.ds(pl.multiple_of(me * lw, 128), lw)] = obuf[me]
    for copy in sends:
        copy.wait_send()
    for d in range(1, n):
        j = lax.rem(me + d, n)
        back = remote(
            obuf.at[j], out_ref.at[:, pl.ds(pl.multiple_of(j * lw, 128), lw)], osend.at[j], orecv.at[j], (j, dp)
        )
        back.wait_send()
        back.wait_recv()


def attention(n, q1, k1, q2, k2, vv, meta, lam, gain, heads):
    rows = q1.shape[0]
    heads_local = heads // n
    hd = q1.shape[1] // heads
    hv = vv.shape[1] // heads
    arrays, sliced = [], []
    for array, width in ((q1, hd), (k1, hd), (q2, hd), (k2, hd), (vv, hv)):
        w = width * heads_local
        good = w % 128 == 0
        arrays.append(array if good else array.reshape(rows, n, w).transpose(1, 0, 2))
        sliced.append(good)
    order = (1, 3, 0, 2, 4)
    w, lw = hd * heads_local, hv * heads_local
    return pl.pallas_call(
        functools.partial(attention_kernel, n, rows, heads_local, hd, hv, [sliced[i] for i in order]),
        out_shape=(
            jax.ShapeDtypeStruct((rows, n * lw), BF16),
            jax.ShapeDtypeStruct((n,) + meta.shape, F32),
        ),
        in_specs=[pl.BlockSpec(memory_space=pltpu.SMEM)]
        + vspec(1)
        + [pl.BlockSpec(memory_space=pl.ANY)] * 5
        + vspec(1),
        out_specs=tuple(vspec(2)),
        scratch_shapes=[VMEM((n, rows, w), BF16)] * 4
        + [VMEM((n, rows, lw), BF16)] * 2
        + [VMEM((heads_local, n * rows, n * rows), F32), VMEM((heads_local, n * rows, n * rows), BF16)]
        + [
            pltpu.SemaphoreType.DMA((6, n)),
            pltpu.SemaphoreType.DMA((6, n)),
            pltpu.SemaphoreType.DMA((6,)),
            pltpu.SemaphoreType.DMA((n,)),
            pltpu.SemaphoreType.DMA((n,)),
        ],
        compiler_params=pltpu.CompilerParams(
            collective_id=0,
            has_side_effects=True,
            vmem_limit_bytes=58 << 20,
        ),
    )(lam, gain, *arrays, meta)


class Place:
    def __init__(self, outer, inner, ndp):
        self.outer, self.inner, self.ndp = outer, inner, ndp
        self.plane = inner * ndp
        sp, self.dp = lax.axis_index("sp"), lax.axis_index("dp")
        self.z, self.y = sp // inner, lax.rem(sp, inner)
        self.me = self.y * ndp + self.dp

    def along(self, z):
        return (z * self.inner + self.y, self.dp)

    def across(self, p):
        return (self.z * self.inner + p // self.ndp, lax.rem(p, self.ndp))

    def all_peers(self):
        peers = [self.along(lax.rem(self.z + d, self.outer)) for d in range(1, self.outer)]
        return peers + [self.across(lax.rem(self.me + d, self.plane)) for d in range(1, self.plane)]

    def order(self):
        tables = [
            sorted(range(self.outer), key=lambda c: (abs(c - z), c if 2 * z < self.outer else -c))
            for z in range(self.outer)
        ]
        steps = []
        for s in range(self.outer):
            value = jnp.int32(tables[0][s])
            for z in range(1, self.outer):
                value = jnp.where(self.z == z, tables[z][s], value)
            steps.append(value)
        return steps


def moe_kernel(
    outer, inner, ndp, parts, x_ref, pick_ref, weigh_ref, mixed_ref, gate_hbm, up_hbm, down_hbm, out_ref,
    gath, staged, recv, hidden, eout, back, from_below, from_above, partial, gate_w, up_w, down_w,
    wsem, gsend, grecv, psend, precv, bsend, brecv, ssend, srecv, own_sem,
):
    at = Place(outer, inner, ndp)
    z, plane = at.z, at.plane
    block, width = recv.shape[2], recv.shape[3]
    held, _, ff = gate_w.shape
    cap = block // held
    piece = width // parts
    spans = [slice(h * piece, (h + 1) * piece) for h in range(parts)]
    order = at.order()
    greet(at.all_peers())
    loads = [
        pltpu.make_async_copy(a, b, wsem.at[i])
        for i, (a, b) in enumerate(((gate_hbm, gate_w), (up_hbm, up_w), (down_hbm, down_w)))
    ]
    own = pltpu.make_async_copy(x_ref, gath.at[z], own_sem)
    own.start()
    own.wait()

    def slab(ref, c, h):
        return ref.at[c, :, spans[h]]

    def up(c, h):
        return remote(
            slab(gath, c, h), slab(gath, c, h), gsend.at[0, c, h], grecv.at[c, h],
            at.along(jnp.minimum(z + 1, outer - 1)),
        )

    def down(c, h):
        return remote(
            slab(gath, c, h), slab(gath, c, h), gsend.at[1, c, h], grecv.at[c, h],
            at.along(jnp.maximum(z - 1, 0)),
        )

    def other(d):
        return lax.rem(at.me + d, plane)

    def out_to(c, d, h):
        p = other(d)
        return remote(
            staged.at[c, p, :, spans[h]], recv.at[c, at.me, :, spans[h]],
            psend.at[c, p, h], precv.at[c, at.me, h], at.across(p),
        )

    def back_to(c, d, h):
        p = other(d)
        return remote(
            eout.at[c, p, :, spans[h]], back.at[c, at.me, :, spans[h]],
            bsend.at[c, p, h], brecv.at[c, at.me, h], at.across(p),
        )

    def chosen(step):
        c = order[0]
        for i in range(1, outer):
            c = jnp.where(step == i, order[i], c)
        return c

    def spread(step):
        c = chosen(step)
        for h in range(parts):

            @pl.when(step > 0)
            def _(h=h):
                remote(
                    slab(gath, c, h), slab(gath, c, h), gsend.at[0, c, h], grecv.at[c, h], at.along(c)
                ).wait_recv()

            @pl.when((c <= z) & (z < outer - 1))
            def _(h=h):
                up(c, h).start()

            @pl.when((c >= z) & (z > 0))
            def _(h=h):
                down(c, h).start()

            rows = gath[c, :, spans[h]]
            for p in range(plane):
                staged[c, p, :, spans[h]] = jnp.dot(
                    pick_ref[c, p * block : (p + 1) * block, :], rows, preferred_element_type=F32
                ).astype(BF16)
            for d in range(1, plane):
                out_to(c, d, h).start()
            recv[c, at.me, :, spans[h]] = staged[c, at.me, :, spans[h]]

    def work(step):
        c = chosen(step)
        for d in range(1, plane):
            p = other(d)
            for h in range(parts):
                remote(
                    staged.at[c, p, :, spans[h]], recv.at[c, p, :, spans[h]],
                    psend.at[c, p, h], precv.at[c, p, h], at.across(p),
                ).wait_recv()

        @pl.when(step == 0)
        def _():
            for load in loads:
                load.wait()

        tile = min(512, ff)
        for e in range(held):
            rows = recv[c, :, e * cap : (e + 1) * cap, :].reshape(plane * cap, width)
            for start in range(0, ff, tile):
                cols = slice(start, start + tile)
                gate = jnp.dot(rows, gate_w[e, :, cols], preferred_element_type=F32)
                upper = jnp.dot(rows, up_w[e, :, cols], preferred_element_type=F32)
                clamped = jnp.minimum(gate, 7.0)
                hidden[e, :, cols] = (
                    (jnp.clip(upper, -7.0, 7.0) + 1.0) * clamped * jax.nn.sigmoid(1.702 * clamped)
                ).astype(BF16)
        tile = min(512, piece)
        for h in range(parts):
            for e in range(held):
                for start in range(h * piece, (h + 1) * piece, tile):
                    cols = slice(start, start + tile)
                    result = jnp.dot(hidden[e], down_w[e, :, cols], preferred_element_type=F32).astype(BF16)
                    eout[c, :, e * cap : (e + 1) * cap, cols] = result.reshape(plane, cap, tile)
            for d in range(1, plane):
                back_to(c, d, h).start()
            back[c, at.me, :, spans[h]] = eout[c, at.me, :, spans[h]]

    def turn(step, carry):
        @pl.when(step < outer)
        def _():
            spread(step)

        @pl.when(step == 0)
        def _():
            for load in loads:
                load.start()

        @pl.when(step > 0)
        def _():
            work(step - 1)

        return carry

    lax.fori_loop(0, outer + 1, turn, 0)

    def rise(c, h):
        return remote(
            slab(partial, c, h), slab(from_below, c, h), ssend.at[c, h], srecv.at[0, c, h],
            at.along(jnp.minimum(z + 1, outer - 1)),
        )

    def fall(c, h):
        return remote(
            slab(partial, c, h), slab(from_above, c, h), ssend.at[c, h], srecv.at[1, c, h],
            at.along(jnp.maximum(z - 1, 0)),
        )

    for step, c in enumerate(order[::-1]):
        weigh = weigh_ref[c]
        below = (c >= z) & (z > 0)
        above = (c <= z) & (z < outer - 1)
        for h in range(parts):
            for d in range(1, plane):
                p = other(d)
                remote(
                    eout.at[c, p, :, spans[h]], back.at[c, p, :, spans[h]],
                    bsend.at[c, p, h], brecv.at[c, p, h], at.across(p),
                ).wait_recv()

            @pl.when(below)
            def _(c=c, h=h):
                remote(
                    slab(partial, c, h), slab(from_below, c, h), ssend.at[c, h], srecv.at[0, c, h], at.along(c)
                ).wait_recv()

            @pl.when(above)
            def _(c=c, h=h):
                remote(
                    slab(partial, c, h), slab(from_above, c, h), ssend.at[c, h], srecv.at[1, c, h], at.along(c)
                ).wait_recv()

            tile = min(512, piece)
            for start in range(h * piece, (h + 1) * piece, tile):
                cols = slice(start, start + tile)
                total = jnp.dot(
                    weigh, back[c, :, :, cols].reshape(plane * block, tile), preferred_element_type=F32
                )
                total = total + jnp.where(below, from_below[c, :, cols].astype(F32), 0.0)
                total = total + jnp.where(above, from_above[c, :, cols].astype(F32), 0.0)
                if step == outer - 1:
                    out_ref[:, cols] = (mixed_ref[:, cols] + total).astype(BF16)
                else:
                    partial[c, :, cols] = total.astype(BF16)
            if step < outer - 1:

                @pl.when(c > z)
                def _(c=c, h=h):
                    rise(c, h).start()

                @pl.when(c < z)
                def _(c=c, h=h):
                    fall(c, h).start()

    for step, c in enumerate(order):
        for h in range(parts):

            @pl.when((c <= z) & (z < outer - 1))
            def _(c=c, h=h):
                up(c, h).wait_send()

            @pl.when((c >= z) & (z > 0))
            def _(c=c, h=h):
                down(c, h).wait_send()

            if step > 0:
                rise(c, h).wait_send()
            for d in range(1, plane):
                out_to(c, d, h).wait_send()
                back_to(c, d, h).wait_send()


def moe(outer, inner, ndp, normed, pick, weigh, mixed, gate_weight, up_weight, down_weight):
    plane = inner * ndp
    rows, width = normed.shape
    block = pick.shape[1] // plane
    held, _, ff = gate_weight.shape
    parts = 4 if width % 512 == 0 else 1
    flat = (outer, plane, block, width)
    line = (outer, rows, width)
    dma = pltpu.SemaphoreType.DMA
    return pl.pallas_call(
        functools.partial(moe_kernel, outer, inner, ndp, parts),
        out_shape=jax.ShapeDtypeStruct((rows, width), BF16),
        in_specs=vspec(4) + [pl.BlockSpec(memory_space=pl.ANY)] * 3,
        out_specs=vspec(1)[0],
        scratch_shapes=[
            VMEM(line, BF16),
            VMEM(flat, BF16),
            VMEM(flat, BF16),
            VMEM((held, plane * (block // held), ff), BF16),
            VMEM(flat, BF16),
            VMEM(flat, BF16),
            VMEM(line, BF16),
            VMEM(line, BF16),
            VMEM(line, BF16),
            VMEM(gate_weight.shape, BF16),
            VMEM(up_weight.shape, BF16),
            VMEM(down_weight.shape, BF16),
            dma((3,)),
            dma((2, outer, parts)),
            dma((outer, parts)),
            dma((outer, plane, parts)),
            dma((outer, plane, parts)),
            dma((outer, plane, parts)),
            dma((outer, plane, parts)),
            dma((outer, parts)),
            dma((2, outer, parts)),
            dma,
        ],
        compiler_params=pltpu.CompilerParams(
            collective_id=1, has_side_effects=True, vmem_limit_bytes=48 << 20
        ),
    )(normed, pick, weigh, mixed, gate_weight, up_weight, down_weight)


def on_device(
    query_first,
    key_first,
    query_second,
    key_second,
    value_rows,
    mix_lambda,
    head_gain,
    residual,
    out_weight,
    norm_gain,
    routes,
    route_weights,
    gate_weight,
    up_weight,
    down_weight,
):
    n, ndp = lax.axis_size("sp"), lax.axis_size("dp")
    rows = query_first.shape[1]
    heads = mix_lambda.shape[0]
    topk = routes.shape[2]
    held = gate_weight.shape[0]
    outer = 1
    while outer * outer < n:
        outer *= 2
    inner = n // outer
    plane = inner * ndp
    experts_all = held * n * ndp
    capacity = max(2, 3 * rows * topk // (2 * experts_all))
    capacity = -(-capacity // 8) * 8
    block = held * capacity

    sp = lax.axis_index("sp")
    local = heads // n
    lam = lax.dynamic_slice_in_dim(mix_lambda, sp * local, local)
    meta = jnp.concatenate([routes[0].astype(F32).T, route_weights[0].T], axis=0)
    head_out, metas = attention(
        n, query_first[0], key_first[0], query_second[0], key_second[0], value_rows[0],
        meta, lam, head_gain[None, :], heads,
    )

    line = lax.dynamic_index_in_dim(
        metas.reshape(outer, inner, 2 * topk, rows), lax.rem(sp, inner), 1, keepdims=False
    )
    ids, weights = line[:, :topk].astype(jnp.int32), line[:, topk:]
    mine = (sp // inner) * plane * held + jnp.arange(plane * held, dtype=jnp.int32)
    named = ids[:, :, None, :] == mine[None, None, :, None]
    member = jnp.any(named, axis=1)
    weight_of = jnp.sum(jnp.where(named, weights[:, :, None, :], 0.0), axis=1)
    before = (jnp.arange(rows)[:, None] < jnp.arange(rows)[None, :]).astype(BF16)
    rank = jnp.einsum("cet,tu->ceu", member.astype(BF16), before, preferred_element_type=F32).astype(jnp.int32)
    slot = member[:, :, None, :] & (rank[:, :, None, :] == jnp.arange(capacity, dtype=jnp.int32)[None, None, :, None])
    pick = slot.astype(BF16).reshape(outer, plane * block, rows)
    weigh = jnp.where(slot, weight_of[:, :, None, :], 0.0).astype(BF16).reshape(outer, plane * block, rows)
    weigh = weigh.transpose(0, 2, 1)

    attn = jnp.dot(head_out, out_weight, preferred_element_type=F32)
    mixed = residual[0].astype(F32) + attn
    normed = (
        mixed * lax.rsqrt(jnp.mean(mixed * mixed, axis=-1, keepdims=True) + 1e-06) * norm_gain
    ).astype(BF16)
    return moe(outer, inner, ndp, normed, pick, weigh, mixed, gate_weight, up_weight, down_weight)[None]


def solution(mesh):
    spread = P("dp", "sp", None)
    split = P(("sp", "dp"), None, None)
    return jax.shard_map(
        on_device,
        mesh=mesh,
        in_specs=(spread,) * 5 + (P(), P(), spread, P(), P(), spread, spread) + (split,) * 3,
        out_specs=spread,
        check_vma=False,
    )
```

profile of v0, /device:TPU:0, one launch (start us, length us, event | category | flops | bytes accessed | tf_op | source)
XLA Modules:
  0.0 179.7 jit_solution(1420843127150364635)
XLA Ops:
  0.0 1.3 dynamic_slice.7.lam_ref
  1.3 0.7 convert_bitcast_fusion
  2.0 1.3 pad_maximum_fusion.meta
  3.3 0.1 eq.40
  3.4 57.8 %shard_map.145 = (bf16[128,2048]{1,0:T(8,128)(2,1)}, f32[8,8,128]{2,1,0:T(8,128)}) custom-call(f32[2]{0:T(128)} %dynamic_slice.7.lam_ref, f32[1,128]{1,0:T(1,128)} %bitcast.42, bf16[128,1024]{1,0:T(8,128)(2,1)} %bitcast.36, bf16[128,1024]{1,0:T(8,128)(2,1)} %bitcast.37, bf16[128,1024]{1,0:T(8,128)(2,1)} %bitcast.38, bf16[128,1024]{1,0:T(8,128)(2,1)} %bitcast.39, ...), custom_call_target="tpu_custom_call" | custom-call | tf_op jit(solution)/shard_map/pallas_call | solution.py:159
  61.2 0.7 dynamic-slice_bitcast_fusion
  61.9 0.1 fusion.1
  62.0 0.1 compare_reduce_fusion
  62.1 0.1 convolution_convert_fusion
  62.2 0.3 copy.24
  62.5 0.1 copy.25
  62.7 0.2 copy.23
  62.9 0.2 fusion
  63.1 0.0 copy-start
  63.2 0.2 copy.26.pick_ref
  63.3 5.0 %multiply_reduce_fusion = (f32[128]{0:T(128)S(1)}, f32[128,2048]{1,0:T(8,128)S(1)}) fusion(bf16[128,2048]{1,0:T(8,128)(2,1)} %get-tuple-element.7, bf16[2048,2048]{1,0:T(8,128)(2,1)} %param.23, bf16[1,128,2048]{2,1,0:T(8,128)(2,1)} %param.22), kind=kOutput, calls=%fused_computation.3 | convolution fusion | flops 1074790272 | bytes 10486272 | tf_op jit(solution)/shard_map/dot_general | solution.py:538
  68.3 0.0 copy-done
  68.3 0.2 multiply_convert_fusion.x_ref
  68.5 110.4 %shard_map.146 = bf16[128,2048]{1,0:T(8,128)(2,1)S(1)} custom-call(bf16[128,2048]{1,0:T(8,128)(2,1)S(1)} %multiply_convert_fusion.x_ref, bf16[4,192,128]{2,1,0:T(8,128)(2,1)S(1)} %copy.26.pick_ref, bf16[4,128,192]{2,1,0:T(8,128)(2,1)S(1)} %get-tuple-element.9.weigh_ref, f32[128,2048]{1,0:T(8,128)S(1)} %get-tuple-element.14.mixed_ref, ...), custom_call_target="tpu_custom_call" | custom-call | tf_op jit(solution)/shard_map/pallas_call | solution.py:447
  178.9 0.8 copy.28
  (8 shorter events, 0.1 us)
Async XLA Ops:
  63.1 5.2 %copy-start = (f32[2048]{0:T(1024)S(1)}, f32[2048]{0:T(1024)}, u32[]{:S(2)}) copy-start(f32[2048]{0:T(1024)} %param.24) | copy-start | bytes 24580
where the time goes:
time: 180 us
  Pallas kernels  168 us (93%)
  matrix products  5.11 us (3%)
  local copies, waits for them, and re-layouts  3.77 us (2%)
  other arithmetic  2.49 us (1%)
    pallas_call x1, Pallas kernels, moe(): pl.pallas_call(functools.partial(moe_kernel, outer, inner, ndp, parts), o...  110 us
    pallas_call x1, Pallas kernels, attention(): pl.pallas_call(functools.partial(attention_kernel, n, rows, heads_local,...  57.8 us
    dot_general x1, matrix products, on_device(): attn = jnp.dot(head_out, out_weight, preferred_element_type=F32)  4.98 us

commit v1 on v0

--- a/solution.py
+++ b/solution.py
@@ -216,10 +216,24 @@
             steps.append(value)
         return steps
 
+    def relays(self):
+        top = self.outer - 1
+        tables = []
+        for z in range(self.outer):
+            late = lambda c, z=z: c + z if c > z else (top - c) + (top - z)
+            tables.append(sorted([c for c in range(self.outer) if c != z], key=late))
+        steps = []
+        for s in range(top):
+            value = jnp.int32(tables[0][s])
+            for z in range(1, self.outer):
+                value = jnp.where(self.z == z, tables[z][s], value)
+            steps.append(value)
+        return steps
+
 
 def moe_kernel(
     outer, inner, ndp, parts, x_ref, pick_ref, weigh_ref, mixed_ref, gate_hbm, up_hbm, down_hbm, out_ref,
-    gath, staged, recv, hidden, eout, back, from_below, from_above, partial, gate_w, up_w, down_w,
+    gath, staged, recv, hidden, eout, back, from_below, from_above, partial, mine, gate_w, up_w, down_w,
     wsem, gsend, grecv, psend, precv, bsend, brecv, ssend, srecv, own_sem,
 ):
     at = Place(outer, inner, ndp)
@@ -230,6 +244,7 @@
     piece = width // parts
     spans = [slice(h * piece, (h + 1) * piece) for h in range(parts)]
     order = at.order()
+    edge = (z == 0) | (z == outer - 1)
     greet(at.all_peers())
     loads = [
         pltpu.make_async_copy(a, b, wsem.at[i])
@@ -277,32 +292,46 @@
             c = jnp.where(step == i, order[i], c)
         return c
 
+    def hand_on(c, h):
+        @pl.when((c <= z) & (z < outer - 1))
+        def _():
+            up(c, h).start()
+
+        @pl.when((c >= z) & (z > 0))
+        def _():
+            down(c, h).start()
+
+    def give(c, h):
+        rows = gath[c, :, spans[h]]
+        for p in range(plane):
+            staged[c, p, :, spans[h]] = jnp.dot(
+                pick_ref[c, p * block : (p + 1) * block, :], rows, preferred_element_type=F32
+            ).astype(BF16)
+        for d in range(1, plane):
+            out_to(c, d, h).start()
+        recv[c, at.me, :, spans[h]] = staged[c, at.me, :, spans[h]]
+
     def spread(step):
-        c = chosen(step)
+        sides = ((z - step, z >= step), (z + step, z + step < outer))
         for h in range(parts):
-
-            @pl.when(step > 0)
-            def _(h=h):
-                remote(
-                    slab(gath, c, h), slab(gath, c, h), gsend.at[0, c, h], grecv.at[c, h], at.along(c)
-                ).wait_recv()
-
-            @pl.when((c <= z) & (z < outer - 1))
-            def _(h=h):
-                up(c, h).start()
-
-            @pl.when((c >= z) & (z > 0))
-            def _(h=h):
-                down(c, h).start()
-
-            rows = gath[c, :, spans[h]]
-            for p in range(plane):
-                staged[c, p, :, spans[h]] = jnp.dot(
-                    pick_ref[c, p * block : (p + 1) * block, :], rows, preferred_element_type=F32
-                ).astype(BF16)
-            for d in range(1, plane):
-                out_to(c, d, h).start()
-            recv[c, at.me, :, spans[h]] = staged[c, at.me, :, spans[h]]
+            for c, there in sides:
+
+                @pl.when(there)
+                def _(c=c, h=h):
+                    remote(
+                        slab(gath, c, h), slab(gath, c, h), gsend.at[0, c, h], grecv.at[c, h], at.along(c)
+                    ).wait_recv()
+                    hand_on(c, h)
+
+            for c, there in sides:
+
+                @pl.when(there)
+                def _(c=c, h=h):
+                    give(c, h)
+
+    def give_back(c, h):
+        for d in range(1, plane):
+            back_to(c, d, h).start()
 
     def work(step):
         c = chosen(step)
@@ -337,27 +366,11 @@
                     cols = slice(start, start + tile)
                     result = jnp.dot(hidden[e], down_w[e, :, cols], preferred_element_type=F32).astype(BF16)
                     eout[c, :, e * cap : (e + 1) * cap, cols] = result.reshape(plane, cap, tile)
-            for d in range(1, plane):
-                back_to(c, d, h).start()
             back[c, at.me, :, spans[h]] = eout[c, at.me, :, spans[h]]
 
-    def turn(step, carry):
-        @pl.when(step < outer)
-        def _():
-            spread(step)
-
-        @pl.when(step == 0)
-        def _():
-            for load in loads:
-                load.start()
-
-        @pl.when(step > 0)
-        def _():
-            work(step - 1)
-
-        return carry
-
-    lax.fori_loop(0, outer + 1, turn, 0)
+            @pl.when((step > 0) & ((step > 1) | jnp.logical_not(edge)))
+            def _(h=h):
+                give_back(c, h)
 
     def rise(c, h):
         return remote(
@@ -371,51 +384,119 @@
             at.along(jnp.maximum(z - 1, 0)),
         )
 
-    for step, c in enumerate(order[::-1]):
-        weigh = weigh_ref[c]
-        below = (c >= z) & (z > 0)
-        above = (c <= z) & (z < outer - 1)
+    def pass_on(c, h):
+        @pl.when(c > z)
+        def _():
+            rise(c, h).start()
+
+        @pl.when(c < z)
+        def _():
+            fall(c, h).start()
+
+    def first(c):
+        return ((c > z) & (z == 0)) | ((c < z) & (z == outer - 1))
+
+    tile = min(512, piece)
+
+    def collect(step, h):
+        c = chosen(step)
+        for d in range(1, plane):
+            p = other(d)
+            remote(
+                eout.at[c, p, :, spans[h]], back.at[c, p, :, spans[h]],
+                bsend.at[c, p, h], brecv.at[c, p, h], at.across(p),
+            ).wait_recv()
+        for start in range(h * piece, (h + 1) * piece, tile):
+            cols = slice(start, start + tile)
+            total = jnp.dot(
+                weigh_ref[c], back[c, :, :, cols].reshape(plane * block, tile), preferred_element_type=F32
+            )
+            mine[c, :, cols] = total
+            partial[c, :, cols] = total.astype(BF16)
+
+        @pl.when(first(c))
+        def _():
+            pass_on(c, h)
+
+    def relay(c, h):
+        @pl.when(jnp.logical_not(first(c)))
+        def _():
+            for side, (here, source) in enumerate(((c > z, from_below), (c < z, from_above))):
+
+                @pl.when(here)
+                def _(side=side, source=source):
+                    remote(
+                        slab(partial, c, h), slab(source, c, h), ssend.at[c, h], srecv.at[side, c, h], at.along(c)
+                    ).wait_recv()
+                    for start in range(h * piece, (h + 1) * piece, tile):
+                        cols = slice(start, start + tile)
+                        partial[c, :, cols] = (mine[c, :, cols] + source[c, :, cols].astype(F32)).astype(BF16)
+
+            pass_on(c, h)
+
+    for h in range(parts):
+        hand_on(z, h)
+    for h in range(parts):
+        give(z, h)
+    for load in loads:
+        load.start()
+
+    def turn(step, carry):
+        @pl.when((step > 0) & (step < outer))
+        def _():
+            spread(step)
+
+        @pl.when((step > 0) & (step <= outer))
+        def _():
+            work(step - 1)
+
+        return carry
+
+    lax.fori_loop(1, outer + 1, turn, 0)
+
+    @pl.when(edge)
+    def _():
+        if outer > 1:
+            for h in range(parts):
+                give_back(order[1], h)
+
+    for h in range(parts):
+        give_back(z, h)
+
+    relays = at.relays()
+    early = outer - 2 if outer == 4 else 0
+    for k in range(outer - 1):
+        step = jnp.where(edge, k + 2 if k < outer - 2 else 1, k + 1)
         for h in range(parts):
-            for d in range(1, plane):
-                p = other(d)
-                remote(
-                    eout.at[c, p, :, spans[h]], back.at[c, p, :, spans[h]],
-                    bsend.at[c, p, h], brecv.at[c, p, h], at.across(p),
-                ).wait_recv()
-
-            @pl.when(below)
-            def _(c=c, h=h):
-                remote(
-                    slab(partial, c, h), slab(from_below, c, h), ssend.at[c, h], srecv.at[0, c, h], at.along(c)
-                ).wait_recv()
-
-            @pl.when(above)
-            def _(c=c, h=h):
-                remote(
-                    slab(partial, c, h), slab(from_above, c, h), ssend.at[c, h], srecv.at[1, c, h], at.along(c)
-                ).wait_recv()
-
-            tile = min(512, piece)
-            for start in range(h * piece, (h + 1) * piece, tile):
-                cols = slice(start, start + tile)
-                total = jnp.dot(
-                    weigh, back[c, :, :, cols].reshape(plane * block, tile), preferred_element_type=F32
-                )
-                total = total + jnp.where(below, from_below[c, :, cols].astype(F32), 0.0)
-                total = total + jnp.where(above, from_above[c, :, cols].astype(F32), 0.0)
-                if step == outer - 1:
-                    out_ref[:, cols] = (mixed_ref[:, cols] + total).astype(BF16)
-                else:
-                    partial[c, :, cols] = total.astype(BF16)
-            if step < outer - 1:
-
-                @pl.when(c > z)
-                def _(c=c, h=h):
-                    rise(c, h).start()
-
-                @pl.when(c < z)
-                def _(c=c, h=h):
-                    fall(c, h).start()
+            collect(step, h)
+            if 0 < k <= early:
+                relay(relays[k - 1], h)
+    for c in relays[early:]:
+        for h in range(parts):
+            relay(c, h)
+    for h in range(parts):
+        collect(0, h)
+    for h in range(parts):
+        @pl.when(z > 0)
+        def _(h=h):
+            remote(
+                slab(partial, z, h), slab(from_below, z, h), ssend.at[z, h], srecv.at[0, z, h],
+                at.along(jnp.maximum(z - 1, 0)),
+            ).wait_recv()
+
+        @pl.when(z < outer - 1)
+        def _(h=h):
+            remote(
+                slab(partial, z, h), slab(from_above, z, h), ssend.at[z, h], srecv.at[1, z, h],
+                at.along(jnp.minimum(z + 1, outer - 1)),
+            ).wait_recv()
+
+        for start in range(h * piece, (h + 1) * piece, tile):
+            cols = slice(start, start + tile)
+            total = mine[z, :, cols] + mixed_ref[:, cols]
+            total = total + jnp.where(z > 0, from_below[z, :, cols].astype(F32), 0.0)
+            total = total + jnp.where(z < outer - 1, from_above[z, :, cols].astype(F32), 0.0)
+            out_ref[:, cols] = total.astype(BF16)
 
     for step, c in enumerate(order):
         for h in range(parts):
@@ -459,6 +540,7 @@
             VMEM(line, BF16),
             VMEM(line, BF16),
             VMEM(line, BF16),
+            VMEM(line, F32),
             VMEM(gate_weight.shape, BF16),
             VMEM(up_weight.shape, BF16),
             VMEM(down_weight.shape, BF16),

time: 180 us -> 157 us (0.87)
  Pallas kernels: 168 us -> 146 us
    pallas_call x1, Pallas kernels: 110 us -> 87.8 us  [moe(): pl.pallas_call(functools.partial(moe_kernel, outer, inner, ndp, parts), o...]
where the time goes in v1:
time: 157 us
  Pallas kernels  146 us (93%)
  matrix products  5.11 us (3%)
  local copies, waits for them, and re-layouts  3.77 us (2%)
  other arithmetic  2.49 us (2%)
    pallas_call x1, Pallas kernels, moe(): pl.pallas_call(functools.partial(moe_kernel, outer, inner, ndp, parts), o...  87.8 us
    pallas_call x1, Pallas kernels, attention(): pl.pallas_call(functools.partial(attention_kernel, n, rows, heads_local,...  57.8 us
    dot_general x1, matrix products, on_device(): attn = jnp.dot(head_out, out_weight, preferred_element_type=F32)  4.98 us

profile of v1, /device:TPU:0, one launch (start us, length us, event | category | flops | bytes accessed | tf_op | source)
XLA Modules:
  0.0 157.1 jit_solution(11818714679754277576)
XLA Ops:
  0.0 1.3 dynamic_slice.7.lam_ref
  1.3 0.7 convert_bitcast_fusion
  2.0 1.3 pad_maximum_fusion.meta
  3.3 0.1 eq.40
  3.4 57.8 %shard_map.145 = (bf16[128,2048]{1,0:T(8,128)(2,1)}, f32[8,8,128]{2,1,0:T(8,128)}) custom-call(f32[2]{0:T(128)} %dynamic_slice.7.lam_ref, f32[1,128]{1,0:T(1,128)} %bitcast.42, bf16[128,1024]{1,0:T(8,128)(2,1)} %bitcast.36, bf16[128,1024]{1,0:T(8,128)(2,1)} %bitcast.37, bf16[128,1024]{1,0:T(8,128)(2,1)} %bitcast.38, bf16[128,1024]{1,0:T(8,128)(2,1)} %bitcast.39, ...), custom_call_target="tpu_custom_call" | custom-call | tf_op jit(solution)/shard_map/pallas_call | solution.py:159
  61.2 0.7 dynamic-slice_bitcast_fusion
  61.9 0.1 fusion.1
  62.0 0.1 compare_reduce_fusion
  62.1 0.1 convolution_convert_fusion
  62.2 0.3 copy.24
  62.5 0.1 copy.25
  62.7 0.2 copy.23
  62.9 0.2 fusion
  63.1 0.0 copy-start
  63.2 0.2 copy.26.pick_ref
  63.3 5.0 %multiply_reduce_fusion = (f32[128]{0:T(128)S(1)}, f32[128,2048]{1,0:T(8,128)S(1)}) fusion(bf16[128,2048]{1,0:T(8,128)(2,1)} %get-tuple-element.7, bf16[2048,2048]{1,0:T(8,128)(2,1)} %param.23, bf16[1,128,2048]{2,1,0:T(8,128)(2,1)} %param.22), kind=kOutput, calls=%fused_computation.3 | convolution fusion | flops 1074790272 | bytes 10486272 | tf_op jit(solution)/shard_map/dot_general | solution.py:620
  68.3 0.0 copy-done
  68.3 0.2 multiply_convert_fusion.x_ref
  68.5 87.8 %shard_map.146 = bf16[128,2048]{1,0:T(8,128)(2,1)S(1)} custom-call(bf16[128,2048]{1,0:T(8,128)(2,1)S(1)} %multiply_convert_fusion.x_ref, bf16[4,192,128]{2,1,0:T(8,128)(2,1)S(1)} %copy.26.pick_ref, bf16[4,128,192]{2,1,0:T(8,128)(2,1)S(1)} %get-tuple-element.9.weigh_ref, f32[128,2048]{1,0:T(8,128)S(1)} %get-tuple-element.14.mixed_ref, ...), custom_call_target="tpu_custom_call" | custom-call | tf_op jit(solution)/shard_map/pallas_call | solution.py:528
  156.3 0.8 copy.28
  (8 shorter events, 0.1 us)
Async XLA Ops:
  63.1 5.2 %copy-start = (f32[2048]{0:T(1024)S(1)}, f32[2048]{0:T(1024)}, u32[]{:S(2)}) copy-start(f32[2048]{0:T(1024)} %param.24) | copy-start | bytes 24580

commit v2 on v1

v2 whole, which is shorter than its diff:
```python
import functools

import jax
import jax.numpy as jnp
from jax import lax
from jax.experimental import pallas as pl
from jax.experimental.pallas import tpu as pltpu
from jax.sharding import PartitionSpec as P

MESH = pl.DeviceIdType.MESH
VMEM = pltpu.VMEM
F32 = jnp.float32
BF16 = jnp.bfloat16


def vspec(number):
    return [pl.BlockSpec(memory_space=VMEM)] * number


def greet(peers):
    barrier = pltpu.get_barrier_semaphore()
    for peer in peers:
        pl.semaphore_signal(barrier, inc=1, device_id=peer, device_id_type=MESH)


def greeted(peers):
    pl.semaphore_wait(pltpu.get_barrier_semaphore(), len(peers))


def remote(src, dst, send_sem, recv_sem, peer):
    return pltpu.make_async_remote_copy(
        src_ref=src, dst_ref=dst, send_sem=send_sem, recv_sem=recv_sem, device_id=peer, device_id_type=MESH
    )


def attention_kernel(
    n, outer, held, rows, heads_local, hd, hv, sliced,
    lam_ref, gain_ref, routes_ref, rw_ref, res_ref, ngain_ref, q1, k1, q2, k2, vv, out_hbm,
    normed_ref, mixed_ref, pick_ref, weigh_ref, out_w,
    b_q1, b_k1, b_q2, b_k2, b_v, obuf, prob, mix, out_ref, meta, meta_out,
    send_sem, recv_sem, local_sem, osend, orecv, wsem,
):
    me, dp = lax.axis_index("sp"), lax.axis_index("dp")
    topk = routes_ref.shape[0]
    ndp, inner = lax.axis_size("dp"), n // outer
    ins = (k1, k2, q1, q2, vv)
    bufs = (b_k1, b_k2, b_q1, b_q2, b_v)
    z, y = me // inner, lax.rem(me, inner)
    peers = [(lax.rem(me + d, n), dp) for d in range(1, n)]
    for d in range(inner):
        peers += [(z * inner + lax.rem(y + d, inner), lax.rem(dp + e, ndp)) for e in range(1, ndp)]
    greet(peers)
    weights = pltpu.make_async_copy(out_hbm, out_w, wsem)
    weights.start()
    down = lax.broadcasted_iota(jnp.int32, (rows, rows), 0)
    over = lax.broadcasted_iota(jnp.int32, (rows, rows), 1)
    eye = (down == over).astype(BF16)
    meta[:topk] = routes_ref[...].astype(F32)
    meta[topk:] = rw_ref[...]
    greeted(peers)

    def part(index, j):
        if not sliced[index]:
            return ins[index].at[j]
        width = bufs[index].shape[2]
        return ins[index].at[:, pl.ds(pl.multiple_of(j * width, 128), width)]

    def move(index, d):
        j = lax.rem(me + d, n)
        if index == 5:
            return remote(meta, meta_out.at[me], send_sem.at[5, d], recv_sem.at[5, me], (j, dp))
        return remote(part(index, j), bufs[index].at[me], send_sem.at[index, d], recv_sem.at[index, me], (j, dp))

    order = (5, 0, 2, 1, 3, 4)
    sends = [move(index, d) for index in order for d in range(1, n)]
    for copy in sends:
        copy.start()
    locals_ = [pltpu.make_async_copy(part(i, me), bufs[i].at[me], local_sem.at[i]) for i in range(5)]
    meta_out[me] = meta[...]
    for copy in locals_:
        copy.start()
    for copy in locals_:
        copy.wait()

    def arrived(index):
        for d in range(1, n):
            j = lax.rem(me + d, n)
            if index == 5:
                remote(meta, meta_out.at[j], send_sem.at[5, d], recv_sem.at[5, j], (j, dp)).wait_recv()
            else:
                remote(
                    part(index, j), bufs[index].at[j], send_sem.at[index, d], recv_sem.at[index, j], (j, dp)
                ).wait_recv()

    group = 2 if n % 2 == 0 else 1
    qb = group * rows
    width = heads_local * hd
    lw = heads_local * hv
    lane = lax.broadcasted_iota(jnp.int32, (1, width), 1) // hd
    scale = hd ** (-0.5)
    blocks = [(i * group, (i + 1) * group) for i in reversed(range(n // group))]

    def softs(lo, hi):
        keys = hi * rows
        at = slice(lo * rows, hi * rows)
        visible = lax.broadcasted_iota(jnp.int32, (qb, keys), 1) <= lo * rows + lax.broadcasted_iota(
            jnp.int32, (qb, keys), 0
        )
        for h in range(heads_local):
            first = None
            for bq, bk in ((b_q1, b_k1), (b_q2, b_k2)):
                query = bq[lo:hi].reshape(qb, width)
                query = jnp.where(lane == h, query, jnp.zeros_like(query))
                key = bk[:hi].reshape(keys, width)
                score = lax.dot_general(query, key, (((1,), (1,)), ((), ())), preferred_element_type=F32) * scale
                score = jnp.where(visible, score, -1e30)
                powers = jnp.exp(score - jnp.max(score, axis=-1, keepdims=True))
                total = jnp.sum(powers, axis=-1, keepdims=True)
                if first is None:
                    first = True
                    prob[:, :keys] = powers * (1.0 / total)
                else:
                    mix[h, at, :keys] = (
                        prob[:, :keys] - powers * (lam_ref[me * heads_local + h] / total)
                    ).astype(BF16)

    def values(lo, hi):
        keys = hi * rows
        for h in range(heads_local):
            value = b_v[:hi, :, h * hv : (h + 1) * hv].reshape(keys, hv)
            raw = jnp.dot(mix[h, lo * rows : hi * rows, :keys], value, preferred_element_type=F32)
            factor = lax.rsqrt(jnp.mean(raw * raw, axis=-1, keepdims=True) + 1e-06)
            done = (raw * factor * gain_ref[...]).astype(BF16)
            obuf[lo:hi, :, h * hv : (h + 1) * hv] = done.reshape(group, rows, hv)
        for j in range(lo, hi):

            @pl.when(j != me)
            def _(j=j):
                remote(
                    obuf.at[j],
                    out_ref.at[:, pl.ds(pl.multiple_of(me * lw, 128), lw)],
                    osend.at[j], orecv.at[me], (j, dp),
                ).start()

    def attend(blocks):
        for i, (lo, hi) in enumerate(blocks):
            softs(lo, hi)
            if i == 0:
                arrived(4)
            values(lo, hi)

    def tables():
        _, slots, _ = pick_ref.shape
        experts = inner * ndp * held
        cap = slots // experts
        name = (z * experts + lax.broadcasted_iota(jnp.int32, (experts, rows), 0)).astype(F32)
        before = (down < over).astype(BF16)
        count = lax.broadcasted_iota(jnp.int32, (experts, cap, rows), 1).astype(F32)
        for c in range(outer):
            line = meta_out[c * inner + y]
            member = jnp.zeros((experts, rows), F32)
            weight = jnp.zeros((experts, rows), F32)
            for t in range(topk):
                named = line[t : t + 1] == name
                member = jnp.where(named, 1.0, member)
                weight = jnp.where(named, line[topk + t : topk + t + 1], weight)
            rank = jnp.dot(member.astype(BF16), before, preferred_element_type=F32)
            rank = jnp.where(member > 0.0, rank, -1.0)
            slot = rank[:, None, :] == count
            pick_ref[c] = jnp.where(slot, 1.0, 0.0).reshape(slots, rows).astype(BF16)
            heavy = jnp.where(slot, weight[:, None, :], 0.0).reshape(slots, rows).astype(BF16)
            weigh_ref[c] = lax.dot_general(
                eye, heavy, (((1,), (1,)), ((), ())), preferred_element_type=F32
            ).astype(BF16)

    arrived(5)
    tables()
    arrived(0)
    arrived(2)
    arrived(1)
    arrived(3)
    lower = 2 * me < n
    pl.when(lower)(lambda: attend(blocks))
    pl.when(jnp.logical_not(lower))(lambda: attend(blocks[::-1]))

    wide = out_w.shape[1]
    tile = min(512, wide)

    def project(j, part_ref, at):
        for start in range(0, wide, tile):
            cols = slice(start, start + tile)
            more = jnp.dot(
                part_ref, out_w[pl.ds(pl.multiple_of(j * lw, 128), lw), cols], preferred_element_type=F32
            )
            mixed_ref[:, cols] = at[:, cols].astype(F32) + more

    weights.wait()
    project(me, obuf[me], res_ref)
    for d in range(1, n):
        j = lax.rem(me + d, n)
        here = pl.ds(pl.multiple_of(j * lw, 128), lw)
        remote(obuf.at[j], out_ref.at[:, here], osend.at[j], orecv.at[j], (j, dp)).wait_recv()
        project(j, out_ref[:, here], mixed_ref)
    square = jnp.zeros((rows, 1), F32)
    for start in range(0, wide, tile):
        chunk = mixed_ref[:, start : start + tile]
        square = square + jnp.sum(chunk * chunk, axis=-1, keepdims=True)
    factor = lax.rsqrt(square * (1.0 / wide) + 1e-06)
    for start in range(0, wide, tile):
        cols = slice(start, start + tile)
        normed_ref[:, cols] = (mixed_ref[:, cols] * factor * ngain_ref[:, cols]).astype(BF16)

    def finish():
        for copy in sends:
            copy.wait_send()
        for d in range(1, n):
            j = lax.rem(me + d, n)
            here = pl.ds(pl.multiple_of(j * lw, 128), lw)
            remote(obuf.at[j], out_ref.at[:, here], osend.at[j], orecv.at[j], (j, dp)).wait_send()

    return finish


class Place:
    def __init__(self, outer, inner, ndp):
        self.outer, self.inner, self.ndp = outer, inner, ndp
        self.plane = inner * ndp
        sp, self.dp = lax.axis_index("sp"), lax.axis_index("dp")
        self.z, self.y = sp // inner, lax.rem(sp, inner)
        self.me = self.y * ndp + self.dp

    def along(self, z):
        return (z * self.inner + self.y, self.dp)

    def across(self, p):
        return (self.z * self.inner + p // self.ndp, lax.rem(p, self.ndp))

    def order(self):
        tables = [
            sorted(range(self.outer), key=lambda c: (abs(c - z), c if 2 * z < self.outer else -c))
            for z in range(self.outer)
        ]
        steps = []
        for s in range(self.outer):
            value = jnp.int32(tables[0][s])
            for z in range(1, self.outer):
                value = jnp.where(self.z == z, tables[z][s], value)
            steps.append(value)
        return steps

    def relays(self):
        top = self.outer - 1
        tables = []
        for z in range(self.outer):
            late = lambda c, z=z: c + z if c > z else (top - c) + (top - z)
            tables.append(sorted([c for c in range(self.outer) if c != z], key=late))
        steps = []
        for s in range(top):
            value = jnp.int32(tables[0][s])
            for z in range(1, self.outer):
                value = jnp.where(self.z == z, tables[z][s], value)
            steps.append(value)
        return steps


def moe_kernel(
    outer, inner, ndp, parts, lots, x_ref, pick_ref, weigh_ref, mixed_ref, gate_hbm, up_hbm, down_hbm, out_ref, pair_w,
    gath, staged, recv, hidden, eout, back, from_below, from_above, partial, mine, down_w,
    wsem, gsend, grecv, psend, precv, bsend, brecv, ssend, srecv,
):
    at = Place(outer, inner, ndp)
    z, plane = at.z, at.plane
    block, width = recv.shape[2], recv.shape[3]
    held, ff, _ = down_w.shape
    cap = block // held
    piece = width // parts
    spans = [slice(h * piece, (h + 1) * piece) for h in range(parts)]
    lot = width // lots
    wide = [slice(g * lot, (g + 1) * lot) for g in range(lots)]
    ratio = parts // lots
    order = at.order()
    edge = (z == 0) | (z == outer - 1)
    gate_w, up_w = pair_w.at[:, :width, :ff], pair_w.at[:, :width, ff : 2 * ff]
    loads = [
        pltpu.make_async_copy(a, b, wsem.at[i])
        for i, (a, b) in enumerate(((gate_hbm, gate_w), (up_hbm, up_w), (down_hbm, down_w)))
    ]
    for load in loads:
        load.start()

    def slab(ref, c, h):
        return ref.at[c, :, spans[h]]

    def up(c, h, src=None):
        return remote(
            slab(gath, c, h) if src is None else src, slab(gath, c, h), gsend.at[0, c, h], grecv.at[c, h],
            at.along(jnp.minimum(z + 1, outer - 1)),
        )

    def down(c, h, src=None):
        return remote(
            slab(gath, c, h) if src is None else src, slab(gath, c, h), gsend.at[1, c, h], grecv.at[c, h],
            at.along(jnp.maximum(z - 1, 0)),
        )

    def other(d):
        return lax.rem(at.me + d, plane)

    def out_to(c, d, g):
        p = other(d)
        return remote(
            staged.at[c, p, :, wide[g]], recv.at[c, at.me, :, wide[g]],
            psend.at[c, p, g], precv.at[c, at.me, g], at.across(p),
        )

    def back_to(c, d, g):
        p = other(d)
        return remote(
            eout.at[c, p, :, wide[g]], back.at[c, at.me, :, wide[g]],
            bsend.at[c, p, g], brecv.at[c, at.me, g], at.across(p),
        )

    def chosen(step):
        c = order[0]
        for i in range(1, outer):
            c = jnp.where(step == i, order[i], c)
        return c

    def hand_on(c, h, src=None):
        @pl.when((c <= z) & (z < outer - 1))
        def _():
            up(c, h, src).start()

        @pl.when((c >= z) & (z > 0))
        def _():
            down(c, h, src).start()

    def sort_out(c, g, rows):
        for p in range(plane):
            staged[c, p, :, wide[g]] = jnp.dot(
                pick_ref[c, p * block : (p + 1) * block, :], rows, preferred_element_type=F32
            ).astype(BF16)

    def give(c, g):
        for d in range(1, plane):
            out_to(c, d, g).start()
        recv[c, at.me, :, wide[g]] = staged[c, at.me, :, wide[g]]

    def spread(step):
        sides = ((z - step, z >= step), (z + step, z + step < outer))
        for h in range(parts):
            for c, there in sides:

                @pl.when(there)
                def _(c=c, h=h):
                    remote(
                        slab(gath, c, h), slab(gath, c, h), gsend.at[0, c, h], grecv.at[c, h], at.along(c)
                    ).wait_recv()
                    hand_on(c, h)

            for c, there in sides if (h + 1) % ratio == 0 else ():

                @pl.when(there)
                def _(c=c, g=h // ratio):
                    sort_out(c, g, gath[c, :, wide[g]])
                    give(c, g)

    def give_back(c, g):
        for d in range(1, plane):
            back_to(c, d, g).start()

    def work(step):
        c = chosen(step)
        for d in range(1, plane):
            p = other(d)
            for g in range(lots):
                remote(
                    staged.at[c, p, :, wide[g]], recv.at[c, p, :, wide[g]],
                    psend.at[c, p, g], precv.at[c, p, g], at.across(p),
                ).wait_recv()

        @pl.when(step == 0)
        def _():
            for load in loads:
                load.wait()

        tile = min(512, ff)
        for e in range(held):
            rows = recv[c, :, e * cap : (e + 1) * cap, :].reshape(plane * cap, width)
            for start in range(0, ff, tile):
                cols = slice(start, start + tile)
                gate = jnp.dot(rows, pair_w[e, :width, start : start + tile], preferred_element_type=F32)
                upper = jnp.dot(rows, pair_w[e, :width, ff + start : ff + start + tile], preferred_element_type=F32)
                clamped = jnp.minimum(gate, 7.0)
                hidden[e, :, cols] = (
                    (jnp.clip(upper, -7.0, 7.0) + 1.0) * clamped * jax.nn.sigmoid(1.702 * clamped)
                ).astype(BF16)
        tile = min(512, piece)
        for g in range(lots):
            for e in range(held):
                for start in range(g * lot, (g + 1) * lot, tile):
                    cols = slice(start, start + tile)
                    result = jnp.dot(hidden[e], down_w[e, :, cols], preferred_element_type=F32).astype(BF16)
                    eout[c, :, e * cap : (e + 1) * cap, cols] = result.reshape(plane, cap, tile)
            back[c, at.me, :, wide[g]] = eout[c, at.me, :, wide[g]]

            @pl.when((step > 0) & ((step > 1) | jnp.logical_not(edge)))
            def _(g=g):
                give_back(c, g)

    def rise(c, h):
        return remote(
            slab(partial, c, h), slab(from_below, c, h), ssend.at[c, h], srecv.at[0, c, h],
            at.along(jnp.minimum(z + 1, outer - 1)),
        )

    def fall(c, h):
        return remote(
            slab(partial, c, h), slab(from_above, c, h), ssend.at[c, h], srecv.at[1, c, h],
            at.along(jnp.maximum(z - 1, 0)),
        )

    def pass_on(c, h):
        @pl.when(c > z)
        def _():
            rise(c, h).start()

        @pl.when(c < z)
        def _():
            fall(c, h).start()

    def first(c):
        return ((c > z) & (z == 0)) | ((c < z) & (z == outer - 1))

    tile = min(512, piece)

    def collect(step, h):
        c = chosen(step)
        g = h // ratio
        for d in range(1, plane) if h % ratio == 0 else ():
            p = other(d)
            remote(
                eout.at[c, p, :, wide[g]], back.at[c, p, :, wide[g]],
                bsend.at[c, p, g], brecv.at[c, p, g], at.across(p),
            ).wait_recv()
        for start in range(h * piece, (h + 1) * piece, tile):
            cols = slice(start, start + tile)
            total = jnp.dot(
                weigh_ref[c], back[c, :, :, cols].reshape(plane * block, tile), preferred_element_type=F32
            )
            mine[c, :, cols] = total
            partial[c, :, cols] = total.astype(BF16)

        @pl.when(first(c))
        def _():
            pass_on(c, h)

    def relay(c, h):
        @pl.when(jnp.logical_not(first(c)))
        def _():
            for side, (here, source) in enumerate(((c > z, from_below), (c < z, from_above))):

                @pl.when(here)
                def _(side=side, source=source):
                    remote(
                        slab(partial, c, h), slab(source, c, h), ssend.at[c, h], srecv.at[side, c, h], at.along(c)
                    ).wait_recv()
                    for start in range(h * piece, (h + 1) * piece, tile):
                        cols = slice(start, start + tile)
                        partial[c, :, cols] = (mine[c, :, cols] + source[c, :, cols].astype(F32)).astype(BF16)

            pass_on(c, h)

    for h in range(parts):
        hand_on(z, h, x_ref.at[:, spans[h]])
    for g in range(lots):
        sort_out(z, g, x_ref[:, wide[g]])
        give(z, g)

    def turn(step, carry):
        @pl.when((step > 0) & (step < outer))
        def _():
            spread(step)

        @pl.when((step > 0) & (step <= outer))
        def _():
            work(step - 1)

        return carry

    lax.fori_loop(1, outer + 1, turn, 0)

    @pl.when(edge)
    def _():
        if outer > 1:
            for g in range(lots):
                give_back(order[1], g)

    for g in range(lots):
        give_back(z, g)

    relays = at.relays()
    early = outer - 2 if outer == 4 else 0
    for k in range(outer - 1):
        step = jnp.where(edge, k + 2 if k < outer - 2 else 1, k + 1)
        for h in range(parts):
            collect(step, h)
            if 0 < k <= early:
                relay(relays[k - 1], h)
    for c in relays[early:]:
        for h in range(parts):
            relay(c, h)
    for h in range(parts):
        collect(0, h)
    for h in range(parts):
        @pl.when(z > 0)
        def _(h=h):
            remote(
                slab(partial, z, h), slab(from_below, z, h), ssend.at[z, h], srecv.at[0, z, h],
                at.along(jnp.maximum(z - 1, 0)),
            ).wait_recv()

        @pl.when(z < outer - 1)
        def _(h=h):
            remote(
                slab(partial, z, h), slab(from_above, z, h), ssend.at[z, h], srecv.at[1, z, h],
                at.along(jnp.minimum(z + 1, outer - 1)),
            ).wait_recv()

        for start in range(h * piece, (h + 1) * piece, tile):
            cols = slice(start, start + tile)
            total = mine[z, :, cols] + mixed_ref[:, cols]
            total = total + jnp.where(z > 0, from_below[z, :, cols].astype(F32), 0.0)
            total = total + jnp.where(z < outer - 1, from_above[z, :, cols].astype(F32), 0.0)
            out_ref[:, cols] = total.astype(BF16)

    for step, c in enumerate(order):
        for h in range(parts):

            @pl.when((c <= z) & (z < outer - 1))
            def _(c=c, h=h):
                up(c, h).wait_send()

            @pl.when((c >= z) & (z > 0))
            def _(c=c, h=h):
                down(c, h).wait_send()

            if step > 0:
                rise(c, h).wait_send()
        for g in range(lots):
            for d in range(1, plane):
                out_to(c, d, g).wait_send()
                back_to(c, d, g).wait_send()


def layer_kernel(n, outer, held, rows, heads_local, hd, hv, sliced, parts, lots, count, *refs):
    small, (gate, up, down), (out,) = refs[:12], refs[12:15], refs[15:16]
    normed, mixed, pick, weigh, pair_w = refs[16:21]
    first, rest = refs[21 : 21 + count], refs[21 + count :]
    wide = out.shape[1]
    finish = attention_kernel(
        n, outer, held, rows, heads_local, hd, hv, sliced, *small,
        normed, mixed, pick, weigh, pair_w.at[0, : n * heads_local * hv, :wide], *first,
    )
    moe_kernel(
        outer, n // outer, lax.axis_size("dp"), parts, lots, normed, pick, weigh, mixed, gate, up, down, out, pair_w, *rest
    )
    finish()


def layer(
    n, outer, capacity, q1, k1, q2, k2, vv, lam, gain, routes, rw, residual, ngain, out_weight,
    gate_weight, up_weight, down_weight,
):
    rows, width = residual.shape
    heads, topk = lam.shape[0], routes.shape[0]
    heads_local = heads // n
    hd = q1.shape[1] // heads
    hv = vv.shape[1] // heads
    held, _, ff = gate_weight.shape
    plane = n // outer * lax.axis_size("dp")
    block = held * capacity
    parts = 4 if width % 512 == 0 else 1
    lots = 2 if parts > 1 else 1
    arrays, sliced = [], []
    for array, each in ((q1, hd), (k1, hd), (q2, hd), (k2, hd), (vv, hv)):
        w = each * heads_local
        good = w % 128 == 0
        arrays.append(array if good else array.reshape(rows, n, w).transpose(1, 0, 2))
        sliced.append(good)
    w, lw = hd * heads_local, hv * heads_local
    group = 2 if n % 2 == 0 else 1
    flat = (outer, plane, block, width)
    line = (outer, rows, width)
    dma = pltpu.SemaphoreType.DMA
    shared = [
        VMEM((rows, width), BF16),
        VMEM((rows, width), F32),
        VMEM((outer, plane * block, rows), BF16),
        VMEM((outer, rows, plane * block), BF16),
        VMEM((held, max(width, n * lw), max(2 * ff, width)), BF16),
    ]
    first = [VMEM((n, rows, w), BF16)] * 4 + [VMEM((n, rows, lw), BF16)] * 2
    first += [
        VMEM((group * rows, n * rows), F32),
        VMEM((heads_local, n * rows, n * rows), BF16),
        VMEM((rows, n * lw), BF16),
        VMEM((2 * topk, rows), F32),
        VMEM((n, 2 * topk, rows), F32),
        dma((6, n)),
        dma((6, n)),
        dma((6,)),
        dma((n,)),
        dma((n,)),
        dma,
    ]
    second = [
        VMEM(line, BF16),
        VMEM(flat, BF16),
        VMEM(flat, BF16),
        VMEM((held, plane * capacity, ff), BF16),
        VMEM(flat, BF16),
        VMEM(flat, BF16),
        VMEM(line, BF16),
        VMEM(line, BF16),
        VMEM(line, BF16),
        VMEM(line, F32),
        VMEM(down_weight.shape, BF16),
        dma((3,)),
        dma((2, outer, parts)),
        dma((outer, parts)),
        dma((outer, plane, lots)),
        dma((outer, plane, lots)),
        dma((outer, plane, lots)),
        dma((outer, plane, lots)),
        dma((outer, parts)),
        dma((2, outer, parts)),
    ]
    order = (1, 3, 0, 2, 4)
    return pl.pallas_call(
        functools.partial(
            layer_kernel, n, outer, held, rows, heads_local, hd, hv, [sliced[i] for i in order], parts, lots, len(first)
        ),
        out_shape=jax.ShapeDtypeStruct((rows, width), BF16),
        in_specs=[pl.BlockSpec(memory_space=pltpu.SMEM)] + vspec(5) + [pl.BlockSpec(memory_space=pl.ANY)] * 9,
        out_specs=vspec(1)[0],
        scratch_shapes=shared + first + second,
        compiler_params=pltpu.CompilerParams(
            collective_id=0, has_side_effects=True, vmem_limit_bytes=63 << 20
        ),
    )(lam, gain, routes, rw, residual, ngain, *arrays, out_weight, gate_weight, up_weight, down_weight)


def on_device(
    query_first,
    key_first,
    query_second,
    key_second,
    value_rows,
    mix_lambda,
    head_gain,
    residual,
    out_weight,
    norm_gain,
    routes,
    route_weights,
    gate_weight,
    up_weight,
    down_weight,
):
    n, ndp = lax.axis_size("sp"), lax.axis_size("dp")
    rows = query_first.shape[1]
    topk = routes.shape[2]
    held = gate_weight.shape[0]
    outer = 1
    while outer * outer < n:
        outer *= 2
    experts_all = held * n * ndp
    capacity = max(2, 3 * rows * topk // (2 * experts_all))
    capacity = -(-capacity // 8) * 8
    return layer(
        n, outer, capacity, query_first[0], key_first[0], query_second[0], key_second[0], value_rows[0],
        mix_lambda, head_gain[None, :], routes[0].T, route_weights[0].T, residual[0], norm_gain[None, :], out_weight,
        gate_weight, up_weight, down_weight,
    )[None]


def solution(mesh):
    spread = P("dp", "sp", None)
    split = P(("sp", "dp"), None, None)
    return jax.shard_map(
        on_device,
        mesh=mesh,
        in_specs=(spread,) * 5 + (P(), P(), spread, P(), P(), spread, spread) + (split,) * 3,
        out_specs=spread,
        check_vma=False,
    )
```

time: 157 us -> 145 us (0.924)
  matrix products: 5.11 us -> 0 us
  Pallas kernels: 146 us -> 142 us
  other arithmetic: 2.49 us -> 0 us
  local copies, waits for them, and re-layouts: 3.77 us -> 1.88 us
    dot_general x2 -> x0, matrix products: 5.11 us -> none  [the longest x1 4.98 us: on_device(): attn = jnp.dot(head_out, out_weight, preferred_element_type=F32)]
    pallas_call x2 -> x1, Pallas kernels: 146 us -> 142 us  [layer(): pl.pallas_call(functools.partial(layer_kernel, n, outer, held, rows, head...]
where the time goes in v2:
time: 145 us; the launch traced here: 144 us
  Pallas kernels  142 us (98%)
  local copies, waits for them, and re-layouts  1.88 us (1%)
    pallas_call x1, Pallas kernels, layer(): pl.pallas_call(functools.partial(layer_kernel, n, outer, held, rows, head...  142 us

profile of v2, /device:TPU:0, one launch (start us, length us, event | category | flops | bytes accessed | tf_op | source)
XLA Modules:
  0.0 144.3 jit_solution(5712795339755797831)
XLA Ops:
  0.0 142.4 %shard_map.145 = bf16[128,2048]{1,0:T(8,128)(2,1)} custom-call(f32[16]{0:T(128)} %refs_0_.1, f32[1,128]{1,0:T(1,128)} %bitcast.25, s32[4,128]{1,0:T(4,128)} %bitcast.23, f32[4,128]{1,0:T(4,128)} %bitcast.24, bf16[128,2048]{1,0:T(8,128)(2,1)} %bitcast.16, f32[1,2048]{1,0:T(1,128)} %bitcast.22, bf16[128,1024]{1,0:T(8,128)(2,1)} %bitcast.18, ...), custom_call_target="tpu_custom_call" | custom-call | tf_op jit(solution)/shard_map/pallas_call | solution.py:640
  142.4 1.9 %copy.17 = bf16[1,128,2048]{2,1,0:T(8,128)(2,1)} copy(bf16[1,128,2048]{2,1,0:T(8,128)(2,1)} %bitcast.15) | data formatting | bytes 1048576
